TPU v7x, 32 devices: a whole 2x2x4 slice. The times are simulated.
32 devices in a mesh: dp: 4 (over y, x), kv: 4 (over z), tp: 2 (over core).
Axes of the slice: x: 2, y: 2, z: 4, core: 2. Of those that a mesh axis runs over, the one named last changes fastest.
Arguments:
- tokens: bfloat16 [16, 4, 2048], P('dp', None, 'kv'), may hold values from -6 to 6
- in_gain: float32 [2048], P('kv'), may hold values from 0.1 to 1.9
- w_gate: bfloat16 [2048, 2048], P('kv', 'tp'), may hold values from -0.125 to 0.125
- w_value: bfloat16 [2048, 2048], P('kv', 'tp'), may hold values from -0.125 to 0.125
- w_key: bfloat16 [2048, 512], P('kv', 'tp'), may hold values from -0.125 to 0.125
- w_query: bfloat16 [2048, 512], P('kv', 'tp'), may hold values from -0.125 to 0.125
- w_step: bfloat16 [2048, 32], P('kv', 'tp'), may hold values from -0.125 to 0.125
- conv_value: bfloat16 [4, 2048], P(None, 'tp'), may hold values from -3 to 3
- conv_key: bfloat16 [4, 512], P(None, 'tp'), may hold values from -3 to 3
- conv_query: bfloat16 [4, 512], P(None, 'tp'), may hold values from -3 to 3
- step_bias: float32 [32], P('tp'), may hold values from -3 to 0
- decay_log: float32 [32], P('tp'), may hold values from -1 to 1.5
- out_gain: float32 [2048], P('tp'), may hold values from 0.1 to 1.9
- w_out: bfloat16 [2048, 2048], P('tp', 'kv'), may hold values from -0.125 to 0.125
- past_value: bfloat16 [16, 7, 2048], P(('dp', 'kv'), None, 'tp'), may hold values from -6 to 6
- past_key: bfloat16 [16, 7, 512], P(('dp', 'kv'), None, 'tp'), may hold values from -6 to 6
- past_query: bfloat16 [16, 7, 512], P(('dp', 'kv'), None, 'tp'), may hold values from -6 to 6
- past_states: float32 [16, 5, 32, 64, 128], P(('dp', 'kv'), None, 'tp'), may hold values from -2 to 2
- accepted: int32 [16], P(('dp', 'kv')), may hold values from 0 to 4
Outputs:
- mixed: bfloat16 [16, 4, 2048], P('dp', None, 'kv')
- new_states: float32 [16, 5, 32, 64, 128], P(('dp', 'kv'), None, 'tp')
- new_value: bfloat16 [16, 7, 2048], P(('dp', 'kv'), None, 'tp')
- new_key: bfloat16 [16, 7, 512], P(('dp', 'kv'), None, 'tp')
- new_query: bfloat16 [16, 7, 512], P(('dp', 'kv'), None, 'tp')
All inputs are finite; a program needn't handle non-finite values.
Results may differ from a plain program's by a relative error of at most 0.014.
Values may be sent and summed in bfloat16 or wider, within the bound.
A program may use at most 64 MiB of HBM per device.

v0:
```python
import functools

import jax
import jax.numpy as jnp
from jax import lax
from jax.experimental import pallas as pl
from jax.experimental.pallas import tpu as pltpu
from jax.sharding import PartitionSpec as P

STATE = 128
EPS = 1e-05
LANES = 128
VMEM_BYTES = 67043328
MESH = pl.DeviceIdType.MESH
F32 = jnp.float32
BF16 = jnp.bfloat16
COMMON = (((1,), (1,)), ((), ()))


def parts_of(x, count):
    found = []
    for _ in range(count):
        piece = x.astype(BF16)
        found.append(piece)
        x = x - piece.astype(F32)
    return found


def silu(x):
    return x / (1.0 + jnp.exp(-x))


def dot(a, b):
    return jnp.dot(a, b, preferred_element_type=F32)


def mixer_kernel(n_kv, n_tp, *refs):
    (tok_h, gain_h, wg_h, wv_h, wk_h, wq_h, ws_h, cv_h, ck_h, cq_h, bias_h, dlog_h, ogain_h, wo_h,
     pv_h, pk_h, pq_h, states_h, acc_h,
     mixed_ref, hist_h, chain_h, convk_h, start_h,
     tok, gain, wg, wv, wk, wq, ws, cv, ck, cq, bias, dlog, ogain, wo, pv, pk, pq, states, acc_ref,
     rows_f, send1, recv1, own1, send2, recv2, own2, expand, shi, slo, gbuf, rows_g, psend, precv, hist_ref, chain, convk, start_v,
     load_sem, out_sem, s1, r1, s2, r2, s3, r3, s4, r4) = refs
    kv = lax.axis_index("kv")
    tp = lax.axis_index("tp")
    n_seq, prop, feat = tok.shape
    own = pv.shape[0]
    rows = n_seq * prop
    width, kwidth, heads = wv.shape[1], wk.shape[1], ws.shape[0]
    head_dim = width // heads
    groups = kwidth // STATE
    gwidth = width // groups
    taps = cv.shape[0]
    cols = wo.shape[1]
    pcols = psend.shape[1] - 2 * LANES
    conv_cols = width + 2 * kwidth

    barrier = pltpu.get_barrier_semaphore()
    for d in range(1, n_kv):
        pl.semaphore_signal(barrier, inc=1, device_id={"kv": lax.rem(kv + d, n_kv)}, device_id_type=MESH)
    for d in range(1, n_tp):
        pl.semaphore_signal(barrier, inc=1, device_id={"tp": lax.rem(tp + d, n_tp)}, device_id_type=MESH)

    pairs = dict(
        tok=(tok_h, tok), gain=(gain_h, gain), ws=(ws_h, ws), wk=(wk_h, wk), wq=(wq_h, wq), wv=(wv_h, wv),
        wg=(wg_h, wg), pv=(pv_h, pv), pk=(pk_h, pk), pq=(pq_h, pq), cv=(cv_h, cv), ck=(ck_h, ck), cq=(cq_h, cq),
        bias=(bias_h, bias), dlog=(dlog_h, dlog), ogain=(ogain_h, ogain), states=(states_h, states), wo=(wo_h, wo), acc=(acc_h, acc_ref),
    )
    loads = {}
    for place, (name, (src, dst)) in enumerate(pairs.items()):
        loads[name] = pltpu.make_async_copy(src, dst, load_sem.at[place])
        loads[name].start()

    row_at = lax.broadcasted_iota(jnp.int32, (LANES, width), 0)
    col_at = lax.broadcasted_iota(jnp.int32, (LANES, width), 1)
    expand[...] = jnp.where(row_at == col_at // head_dim, 1.0, 0.0).astype(BF16)
    lane = lax.broadcasted_iota(jnp.int32, (rows, LANES), 1)

    loads["tok"].wait()
    loads["gain"].wait()
    for s in range(n_seq):
        rows_f[s * prop:(s + 1) * prop, :] = tok[s].astype(F32)
    x = rows_f[...]
    normed = (x * gain[...].reshape(1, feat)).astype(BF16)
    squares = jnp.sum(x * x, axis=1, keepdims=True)

    def stage(product, send, kept, at):
        n = product.shape[1]
        for s in range(n_seq):
            piece = product[s * prop:(s + 1) * prop]
            kept[s, :, at:at + n] = piece
            send[s, :, at:at + n] = piece.astype(BF16)

    loads["ws"].wait()
    step_part = lax.dot_general(normed, ws[...], COMMON, preferred_element_type=F32)
    rows_g[:, 0:LANES] = jnp.zeros((rows, LANES), F32)
    rows_g[:, 0:heads] = step_part
    stat = jnp.where(lane == heads, squares, rows_g[:, 0:LANES])
    stat_hi, stat_lo = parts_of(stat, 2)
    for s in range(n_seq):
        own1[s, :, conv_cols:conv_cols + LANES] = stat[s * prop:(s + 1) * prop]
        send1[s, :, conv_cols:conv_cols + LANES] = stat_hi.astype(F32)[s * prop:(s + 1) * prop].astype(BF16)
        send1[s, :, conv_cols + LANES:] = stat_lo.astype(F32)[s * prop:(s + 1) * prop].astype(BF16)
    loads["wk"].wait()
    stage(dot(normed, wk[...]), send1, own1, width)
    loads["wq"].wait()
    stage(dot(normed, wq[...]), send1, own1, width + kwidth)
    loads["wv"].wait()
    stage(dot(normed, wv[...]), send1, own1, 0)

    pl.semaphore_wait(barrier, n_kv - 1 + n_tp - 1)

    def scatter(send, recv, send_sem, recv_sem):
        copies = []
        for d in range(1, n_kv):
            peer = lax.rem(kv + d, n_kv)
            copies.append(pltpu.make_async_remote_copy(
                src_ref=send.at[pl.ds(peer * own, own)], dst_ref=recv.at[d - 1],
                send_sem=send_sem.at[d - 1], recv_sem=recv_sem.at[d - 1],
                device_id={"kv": peer}, device_id_type=MESH))
        order = sorted(range(n_kv - 1), key=lambda i: -min(i + 1, n_kv - 1 - i))
        for i in order:
            copies[i].start()
        return copies

    first = scatter(send1, recv1, s1, r1)
    loads["wg"].wait()
    stage(dot(normed, wg[...]), send2, own2, 0)
    second = scatter(send2, recv2, s2, r2)

    for name in ("acc", "pv", "pk", "pq", "cv", "ck", "cq", "bias", "dlog", "ogain"):
        loads[name].wait()
    span = taps - 1
    for j in range(own):
        chosen = acc_ref[j]
        at = 0
        for past in (pv, pk, pq):
            wide = past[j].astype(F32)
            window = wide[0:span]
            for a in range(1, wide.shape[0] - span + 1):
                window = jnp.where(chosen == a, wide[a:a + span], window)
            hist_ref[j, 0:span, at:at + wide.shape[1]] = window
            at += wide.shape[1]
    rate = -jnp.exp(dlog[...].reshape(1, heads))
    each = lax.broadcasted_iota(jnp.int32, (8, heads), 0)
    known = jnp.where(each == 0, bias[...].reshape(1, heads), jnp.where(each == 1, rate, 0.0))
    spread = sum(dot(piece, expand[0:heads, :]) for piece in parts_of(known, 3))
    bias_e, rate_e = spread[0:1], spread[1:2]
    taps_v, taps_k, taps_q = (c[...].astype(F32) for c in (cv, ck, cq))
    gain_out = ogain[...].reshape(1, width)
    loads["states"].wait()
    for j in range(own):
        start = states[j, acc_ref[j]]
        start_v[j] = start
        start = start.reshape(width, STATE)
        hi, lo = parts_of(start, 2)
        shi[j] = hi
        slo[j] = lo

    for copy in first:
        copy.wait()
    t_at = lax.broadcasted_iota(jnp.int32, (prop, width), 0)
    results = []
    for j in range(own):
        mine = kv * own + j
        total = own1[mine]
        sums = total[:, 0:conv_cols]
        stats = total[:, conv_cols:conv_cols + LANES]
        for d in range(n_kv - 1):
            got = recv1[d, j].astype(F32)
            sums = sums + got[:, 0:conv_cols]
            stats = stats + got[:, conv_cols:conv_cols + LANES] + got[:, conv_cols + LANES:]
        rscale = lax.rsqrt(stats[:, heads:heads + 1] / (feat * n_kv) + EPS)
        raw = stats[:, 0:heads] * rscale
        raw_e = sum(dot(piece, expand[0:heads, :]) for piece in parts_of(raw, 3))
        hist_ref[j, span:span + prop, :] = (sums * rscale).astype(BF16).astype(F32)

        def conv(c, at, n):
            total = hist_ref[j, 0:prop, at:at + n] * c[0:1]
            for i in range(1, taps):
                total = total + hist_ref[j, i:i + prop, at:at + n] * c[i:i + 1]
            return silu(total)

        conv_k = conv(taps_k, width, kwidth)
        conv_q = conv(taps_q, width + kwidth, kwidth)
        conv_v = conv(taps_v, 0, width)
        pre = raw_e + bias_e
        dt = jnp.maximum(pre, 0.0) + jnp.log1p(jnp.exp(-jnp.abs(pre)))
        logd = dt * rate_e
        moved = dt * conv_v
        chain[j, 0:prop, :] = moved
        chain[j, prop:2 * prop, :] = jnp.exp(logd)
        convk[j] = conv_k
        cum = jnp.zeros_like(logd)
        for s in range(prop):
            cum = cum + jnp.where(t_at >= s, logd[s:s + 1], 0.0)
        parts = []
        for g in range(groups):
            qg = conv_q[:, g * STATE:(g + 1) * STATE]
            kg = conv_k[:, g * STATE:(g + 1) * STATE]
            q_hi, q_lo = parts_of(qg, 2)
            s_hi = shi[j, g * gwidth:(g + 1) * gwidth, :]
            s_lo = slo[j, g * gwidth:(g + 1) * gwidth, :]
            read = functools.partial(lax.dot_general, dimension_numbers=COMMON, preferred_element_type=F32)
            y = read(q_hi, s_hi) + read(q_lo, s_hi) + read(q_hi, s_lo)
            lo_at = g * gwidth
            cum_g = cum[:, lo_at:lo_at + gwidth]
            y = y * jnp.exp(cum_g)
            for s in range(prop):
                kq = jnp.sum(qg * kg[s:s + 1], axis=1, keepdims=True)
                weight = jnp.exp(jnp.where(t_at[:, 0:gwidth] >= s, cum_g - cum_g[s:s + 1], -jnp.inf))
                y = y + weight * (moved[s:s + 1, lo_at:lo_at + gwidth] * kq)
            parts.append(y)
        results.append((jnp.concatenate(parts, axis=1), rscale))

    for copy in second:
        copy.wait()
    for j in range(own):
        mine = kv * own + j
        y, rscale = results[j]
        total = own2[mine]
        for d in range(n_kv - 1):
            total = total + recv2[d, j].astype(F32)
        gate = (total * rscale).astype(BF16).astype(F32)
        gated = y * silu(gate)
        sq_hi, sq_lo = parts_of(jnp.broadcast_to(jnp.sum(gated * gated, axis=1, keepdims=True), (prop, LANES)), 2)
        gbuf[mine, :, 0:width] = (gated * gain_out).astype(BF16)
        gbuf[mine, :, width:width + LANES] = sq_hi
        gbuf[mine, :, width + LANES:] = sq_lo

    gathers = []
    for d in range(1, n_kv):
        peer = lax.rem(kv + d, n_kv)
        gathers.append(pltpu.make_async_remote_copy(
            src_ref=gbuf.at[pl.ds(kv * own, own)], dst_ref=gbuf.at[pl.ds(kv * own, own)],
            send_sem=s3.at[d - 1], recv_sem=r3.at[d - 1],
            device_id={"kv": peer}, device_id_type=MESH))
    for i in sorted(range(n_kv - 1), key=lambda i: -min(i + 1, n_kv - 1 - i)):
        gathers[i].start()
    stores = [pltpu.make_async_copy(src, dst, out_sem.at[i]) for i, (src, dst) in enumerate(
        ((start_v, start_h), (hist_ref, hist_h), (chain, chain_h), (convk, convk_h)))]
    for store in stores:
        store.start()
    loads["wo"].wait()
    for i, copy in enumerate(gathers):
        copy.wait()
    for s in range(n_seq):
        rows_g[s * prop:(s + 1) * prop, :] = gbuf[s].astype(F32)
    outn = rows_g[:, 0:width].astype(BF16)
    psend[:, 0:cols] = dot(outn, wo[...]).astype(BF16)
    psend[:, pcols:pcols + LANES] = rows_g[:, width:width + LANES].astype(BF16)
    psend[:, pcols + LANES:] = rows_g[:, width + LANES:].astype(BF16)
    swaps = []
    for d in range(1, n_tp):
        swaps.append(pltpu.make_async_remote_copy(
            src_ref=psend, dst_ref=precv.at[d - 1], send_sem=s4.at[d - 1], recv_sem=r4.at[d - 1],
            device_id={"tp": lax.rem(tp + d, n_tp)}, device_id_type=MESH))
        swaps[-1].start()
    total = psend[:, 0:cols].astype(F32)
    square = rows_g[:, width:width + 1] + rows_g[:, width + LANES:width + LANES + 1]
    for d, copy in enumerate(swaps):
        copy.wait()
        total = total + precv[d, :, 0:cols].astype(F32)
        square = square + precv[d, :, pcols:pcols + 1].astype(F32)
        square = square + precv[d, :, pcols + LANES:pcols + LANES + 1].astype(F32)
    mixed = total * lax.rsqrt(square / (width * n_tp) + EPS)
    for s in range(n_seq):
        mixed_ref[s] = mixed[s * prop:(s + 1) * prop].astype(BF16)
    for store in stores:
        store.wait()


def states_kernel(chunk, mixed_h, hist_h, chain_h, convk_h, start_h,
                  mixed_ref, new_h, nv_ref, nk_ref, nq_ref,
                  mixed, hist, chain, convk, buf, cols_t, in_sem, load_sem, out_sem):
    own, keep, heads, head_dim, state = buf.shape
    steps = keep - 1
    per_group = heads // (convk.shape[2] // state)
    chunks = heads // chunk
    small = [pltpu.make_async_copy(src, dst, in_sem.at[i]) for i, (src, dst) in enumerate(
        ((chain_h, chain), (convk_h, convk), (hist_h, hist), (mixed_h, mixed)))]
    loads = [[pltpu.make_async_copy(
        start_h.at[j, pl.ds(c * chunk, chunk)], buf.at[j, 0, pl.ds(c * chunk, chunk)],
        load_sem.at[j, c]) for c in range(chunks)] for j in range(own)]
    for copy in small[:2]:
        copy.start()
    for j in range(own):
        for c in range(chunks):
            loads[j][c].start()
    for copy in small[2:]:
        copy.start()
    for copy in small[:2]:
        copy.wait()
    stores = []
    for j in range(own):
        cols_t[...] = jnp.transpose(chain[j])
        for c in range(chunks):
            loads[j][c].wait()
            for h in range(c * chunk, (c + 1) * chunk):
                s = buf[j, 0, h]
                g = h // per_group
                at = h * head_dim
                for t in range(steps):
                    lift = cols_t[at:at + head_dim, t:t + 1]
                    fade = cols_t[at:at + 1, steps + t:steps + t + 1]
                    s = s * fade + lift * convk[j, t:t + 1, g * state:(g + 1) * state]
                    buf[j, t + 1, h] = s
            out = pltpu.make_async_copy(
                buf.at[j, :, pl.ds(c * chunk, chunk)], new_h.at[j, :, pl.ds(c * chunk, chunk)], out_sem.at[j, c])
            out.start()
            stores.append(out)
    for copy in small[2:]:
        copy.wait()
    mixed_ref[...] = mixed[...]
    at = 0
    for ref in (nv_ref, nk_ref, nq_ref):
        n = ref.shape[2]
        for j in range(own):
            ref[j] = hist[j, 0:ref.shape[1], at:at + n].astype(BF16)
        at += n
    for out in stores:
        out.wait()


def per_device(n_kv, n_tp, *args):
    (tokens, in_gain, w_gate, w_value, w_key, w_query, w_step, conv_value, conv_key, conv_query, step_bias,
     decay_log, out_gain, w_out, past_value, past_key, past_query, past_states, accepted) = args
    n_seq, prop, feat = tokens.shape
    own, keep, heads, head_dim, state = past_states.shape
    width, kwidth, cols = w_value.shape[1], w_key.shape[1], w_out.shape[1]
    conv_cols = width + 2 * kwidth
    wide1 = conv_cols + 2 * LANES
    gcols = width + 2 * LANES
    pcols = -(-cols // LANES) * LANES + 2 * LANES
    rows = n_seq * prop
    hist_rows = past_value.shape[1]
    vmem = pl.BlockSpec(memory_space=pltpu.VMEM)
    hbm = pl.BlockSpec(memory_space=pltpu.HBM)
    dma = pltpu.SemaphoreType.DMA
    args = args[:6] + (w_step.T,) + args[7:]
    held = [pltpu.VMEM(a.shape, a.dtype) for a in args[:-1]] + [pltpu.SMEM(accepted.shape, accepted.dtype)]
    peers = n_kv - 1
    passed = (
        jax.ShapeDtypeStruct((n_seq, prop, cols), BF16),
        jax.ShapeDtypeStruct((own, hist_rows, conv_cols), F32),
        jax.ShapeDtypeStruct((own, 2 * prop, width), F32),
        jax.ShapeDtypeStruct((own, prop, kwidth), F32),
        jax.ShapeDtypeStruct((own, heads, head_dim, state), F32),
    )
    kept = [pltpu.VMEM(a.shape, a.dtype) for a in passed]
    handed = pl.pallas_call(
        functools.partial(mixer_kernel, n_kv, n_tp),
        out_shape=passed,
        in_specs=[hbm] * 19,
        out_specs=(vmem,) + (hbm,) * 4,
        scratch_shapes=held + [
            pltpu.VMEM((rows, feat), F32),
            pltpu.VMEM((n_seq, prop, wide1), BF16),
            pltpu.VMEM((peers, own, prop, wide1), BF16),
            pltpu.VMEM((n_seq, prop, conv_cols + LANES), F32),
            pltpu.VMEM((n_seq, prop, width), BF16),
            pltpu.VMEM((peers, own, prop, width), BF16),
            pltpu.VMEM((n_seq, prop, width), F32),
            pltpu.VMEM((LANES, width), BF16),
            pltpu.VMEM((own, width, state), BF16),
            pltpu.VMEM((own, width, state), BF16),
            pltpu.VMEM((n_seq, prop, gcols), BF16),
            pltpu.VMEM((rows, gcols), F32),
            pltpu.VMEM((rows, pcols), BF16),
            pltpu.VMEM((n_tp - 1, rows, pcols), BF16),
        ] + kept[1:] + [
            dma((19,)), dma((4,)),
            dma((peers,)), dma((peers,)), dma((peers,)), dma((peers,)), dma((peers,)), dma((peers,)),
            dma((n_tp - 1,)), dma((n_tp - 1,)),
        ],
        compiler_params=pltpu.CompilerParams(
            collective_id=0, has_side_effects=True, vmem_limit_bytes=VMEM_BYTES),
        name="mixer",
    )(*args)
    chunk = 4 if heads % 4 == 0 else 1
    mixed, new_states, new_value, new_key, new_query = pl.pallas_call(
        functools.partial(states_kernel, chunk),
        out_shape=passed[:1] + tuple(
            jax.ShapeDtypeStruct(a.shape, a.dtype) for a in (past_states, past_value, past_key, past_query)),
        in_specs=[hbm] * 5,
        out_specs=(vmem, hbm, vmem, vmem, vmem),
        scratch_shapes=kept[:4] + [
            pltpu.VMEM(past_states.shape, F32),
            pltpu.VMEM((width, 2 * prop), F32),
            dma((4,)), dma((own, heads // chunk)), dma((own, heads // chunk)),
        ],
        compiler_params=pltpu.CompilerParams(vmem_limit_bytes=VMEM_BYTES),
        name="states",
    )(*handed)
    return (mixed, new_states, new_value, new_key, new_query)


def solution(mesh):
    seqs = ("dp", "kv")
    placed = (
        P("dp", None, "kv"), P("kv"),
        P("kv", "tp"), P("kv", "tp"), P("kv", "tp"), P("kv", "tp"), P("kv", "tp"),
        P(None, "tp"), P(None, "tp"), P(None, "tp"),
        P("tp"), P("tp"), P("tp"), P("tp", "kv"),
        P(seqs, None, "tp"), P(seqs, None, "tp"), P(seqs, None, "tp"),
        P(seqs, None, "tp", None, None), P(seqs),
    )
    return jax.shard_map(
        functools.partial(per_device, mesh.shape["kv"], mesh.shape["tp"]),
        mesh=mesh,
        in_specs=placed,
        out_specs=(
            P("dp", None, "kv"),
            P(seqs, None, "tp", None, None),
            P(seqs, None, "tp"), P(seqs, None, "tp"), P(seqs, None, "tp"),
        ),
        check_vma=False,
    )
```

profile of v0, /device:TPU:0, one launch (start us, length us, event | category | flops | bytes accessed | tf_op | source)
XLA Modules:
  0.0 20.4 jit_solution(16463602064845804906)
XLA Ops:
  1.3 15.5 %mixer.1 = (bf16[4,4,512]{2,1,0:T(4,128)(2,1)}, f32[1,7,1536]{2,1,0:T(8,128)}, f32[1,8,1024]{2,1,0:T(8,128)}, f32[1,4,256]{2,1,0:T(4,128)}, f32[1,16,64,128]{3,2,1,0:T(8,128)}) custom-call(bf16[4,4,512]{2,1,0:T(4,128)(2,1)} %refs_0_.1, f32[512]{0:T(512)} %refs_1_.1, bf16[512,1024]{1,0:T(8,128)(2,1)} %refs_2_.1, bf16[512,1024]{1,0:T(8,128)(2,1)} %refs_3_.1, ...), custom_call_target="tpu_custom_call" | custom-call | tf_op jit(solution)/shard_map/mixer/pallas_call | solution.py:351
  16.8 3.6 %states.1 = (bf16[4,4,512]{2,1,0:T(4,128)(2,1)}, f32[1,5,16,64,128]{4,3,2,1,0:T(8,128)}, bf16[1,7,1024]{2,1,0:T(8,128)(2,1)}, bf16[1,7,256]{2,1,0:T(8,128)(2,1)}, bf16[1,7,256]{2,1,0:T(8,128)(2,1)}) custom-call(bf16[4,4,512]{2,1,0:T(4,128)(2,1)} %get-tuple-element.10.mixed_h, f32[1,7,1536]{2,1,0:T(8,128)} %get-tuple-element.11.hist_h, ...), custom_call_target="tpu_custom_call" | custom-call | tf_op jit(solution)/shard_map/states/pallas_call | solution.py:381
where the time goes:
time: 20.6 us; the launch traced here: 20.4 us
  Pallas kernels  19.1 us (93%)
  between operations  1.29 us (6%)
    pallas_call x1, Pallas kernels, per_device(): pl.pallas_call(functools.partial(mixer_kernel, n_kv, n_tp), out_shape=pas...  15.5 us
    pallas_call x1, Pallas kernels, per_device(): pl.pallas_call(functools.partial(states_kernel, chunk), out_shape=passed[...  3.59 us

commit v1 on v0

--- a/solution.py
+++ b/solution.py
@@ -10,6 +10,7 @@
 STATE = 128
 EPS = 1e-05
 LANES = 128
+HALF = LANES // 2
 VMEM_BYTES = 67043328
 MESH = pl.DeviceIdType.MESH
 F32 = jnp.float32
@@ -52,7 +53,7 @@
     gwidth = width // groups
     taps = cv.shape[0]
     cols = wo.shape[1]
-    pcols = psend.shape[1] - 2 * LANES
+    pcols = psend.shape[1] - LANES
     conv_cols = width + 2 * kwidth
 
     barrier = pltpu.get_barrier_semaphore()
@@ -96,11 +97,11 @@
     rows_g[:, 0:LANES] = jnp.zeros((rows, LANES), F32)
     rows_g[:, 0:heads] = step_part
     stat = jnp.where(lane == heads, squares, rows_g[:, 0:LANES])
-    stat_hi, stat_lo = parts_of(stat, 2)
+    stat_hi = stat.astype(BF16).astype(F32)
+    packed = stat_hi + pltpu.roll(stat - stat_hi, HALF, 1)
     for s in range(n_seq):
-        own1[s, :, conv_cols:conv_cols + LANES] = stat[s * prop:(s + 1) * prop]
-        send1[s, :, conv_cols:conv_cols + LANES] = stat_hi.astype(F32)[s * prop:(s + 1) * prop].astype(BF16)
-        send1[s, :, conv_cols + LANES:] = stat_lo.astype(F32)[s * prop:(s + 1) * prop].astype(BF16)
+        own1[s, :, conv_cols:] = stat[s * prop:(s + 1) * prop]
+        send1[s, :, conv_cols:] = packed[s * prop:(s + 1) * prop].astype(BF16)
     loads["wk"].wait()
     stage(dot(normed, wk[...]), send1, own1, width)
     loads["wq"].wait()
@@ -165,11 +166,11 @@
         mine = kv * own + j
         total = own1[mine]
         sums = total[:, 0:conv_cols]
-        stats = total[:, conv_cols:conv_cols + LANES]
+        stats = total[:, conv_cols:]
         for d in range(n_kv - 1):
             got = recv1[d, j].astype(F32)
             sums = sums + got[:, 0:conv_cols]
-            stats = stats + got[:, conv_cols:conv_cols + LANES] + got[:, conv_cols + LANES:]
+            stats = stats + got[:, conv_cols:] + pltpu.roll(got[:, conv_cols:], HALF, 1)
         rscale = lax.rsqrt(stats[:, heads:heads + 1] / (feat * n_kv) + EPS)
         raw = stats[:, 0:heads] * rscale
         raw_e = sum(dot(piece, expand[0:heads, :]) for piece in parts_of(raw, 3))
@@ -223,10 +224,10 @@
             total = total + recv2[d, j].astype(F32)
         gate = (total * rscale).astype(BF16).astype(F32)
         gated = y * silu(gate)
-        sq_hi, sq_lo = parts_of(jnp.broadcast_to(jnp.sum(gated * gated, axis=1, keepdims=True), (prop, LANES)), 2)
+        square = jnp.sum(gated * gated, axis=1, keepdims=True)
+        square_hi = square.astype(BF16).astype(F32)
         gbuf[mine, :, 0:width] = (gated * gain_out).astype(BF16)
-        gbuf[mine, :, width:width + LANES] = sq_hi
-        gbuf[mine, :, width + LANES:] = sq_lo
+        gbuf[mine, :, width:] = jnp.where(lane[0:prop] == 0, square_hi, square - square_hi).astype(BF16)
 
     gathers = []
     for d in range(1, n_kv):
@@ -248,8 +249,7 @@
         rows_g[s * prop:(s + 1) * prop, :] = gbuf[s].astype(F32)
     outn = rows_g[:, 0:width].astype(BF16)
     psend[:, 0:cols] = dot(outn, wo[...]).astype(BF16)
-    psend[:, pcols:pcols + LANES] = rows_g[:, width:width + LANES].astype(BF16)
-    psend[:, pcols + LANES:] = rows_g[:, width + LANES:].astype(BF16)
+    psend[:, pcols:] = rows_g[:, width:].astype(BF16)
     swaps = []
     for d in range(1, n_tp):
         swaps.append(pltpu.make_async_remote_copy(
@@ -257,12 +257,12 @@
             device_id={"tp": lax.rem(tp + d, n_tp)}, device_id_type=MESH))
         swaps[-1].start()
     total = psend[:, 0:cols].astype(F32)
-    square = rows_g[:, width:width + 1] + rows_g[:, width + LANES:width + LANES + 1]
+    square = rows_g[:, width:width + 1] + rows_g[:, width + 1:width + 2]
     for d, copy in enumerate(swaps):
         copy.wait()
         total = total + precv[d, :, 0:cols].astype(F32)
-        square = square + precv[d, :, pcols:pcols + 1].astype(F32)
-        square = square + precv[d, :, pcols + LANES:pcols + LANES + 1].astype(F32)
+        extra = precv[d, :, pcols:].astype(F32)
+        square = square + extra[:, 0:1] + extra[:, 1:2]
     mixed = total * lax.rsqrt(square / (width * n_tp) + EPS)
     for s in range(n_seq):
         mixed_ref[s] = mixed[s * prop:(s + 1) * prop].astype(BF16)
@@ -271,8 +271,8 @@
 
 
 def states_kernel(chunk, mixed_h, hist_h, chain_h, convk_h, start_h,
-                  mixed_ref, new_h, nv_ref, nk_ref, nq_ref,
-                  mixed, hist, chain, convk, buf, cols_t, in_sem, load_sem, out_sem):
+                  mixed_out, new_h, nv_h, nk_h, nq_h,
+                  mixed, hist, chain, convk, buf, cols_t, nv, nk, nq, in_sem, load_sem, out_sem, end_sem):
     own, keep, heads, head_dim, state = buf.shape
     steps = keep - 1
     per_group = heads // (convk.shape[2] // state)
@@ -291,7 +291,7 @@
         copy.start()
     for copy in small[:2]:
         copy.wait()
-    stores = []
+    stores, ends = [], []
     for j in range(own):
         cols_t[...] = jnp.transpose(chain[j])
         for c in range(chunks):
@@ -309,16 +309,20 @@
                 buf.at[j, :, pl.ds(c * chunk, chunk)], new_h.at[j, :, pl.ds(c * chunk, chunk)], out_sem.at[j, c])
             out.start()
             stores.append(out)
-    for copy in small[2:]:
-        copy.wait()
-    mixed_ref[...] = mixed[...]
-    at = 0
-    for ref in (nv_ref, nk_ref, nq_ref):
-        n = ref.shape[2]
-        for j in range(own):
-            ref[j] = hist[j, 0:ref.shape[1], at:at + n].astype(BF16)
-        at += n
-    for out in stores:
+            if not ends:
+                for copy in small[2:]:
+                    copy.wait()
+                at = 0
+                for ref in (nv, nk, nq):
+                    n = ref.shape[2]
+                    for i in range(own):
+                        ref[i] = hist[i, 0:ref.shape[1], at:at + n].astype(BF16)
+                    at += n
+                ends = [pltpu.make_async_copy(src, dst, end_sem.at[i]) for i, (src, dst) in enumerate(
+                    ((mixed, mixed_out), (nv, nv_h), (nk, nk_h), (nq, nq_h)))]
+                for end in ends:
+                    end.start()
+    for out in stores + ends:
         out.wait()
 
 
@@ -329,9 +333,9 @@
     own, keep, heads, head_dim, state = past_states.shape
     width, kwidth, cols = w_value.shape[1], w_key.shape[1], w_out.shape[1]
     conv_cols = width + 2 * kwidth
-    wide1 = conv_cols + 2 * LANES
-    gcols = width + 2 * LANES
-    pcols = -(-cols // LANES) * LANES + 2 * LANES
+    wide1 = conv_cols + LANES
+    gcols = width + LANES
+    pcols = -(-cols // LANES) * LANES + LANES
     rows = n_seq * prop
     hist_rows = past_value.shape[1]
     vmem = pl.BlockSpec(memory_space=pltpu.VMEM)
@@ -383,11 +387,12 @@
         out_shape=passed[:1] + tuple(
             jax.ShapeDtypeStruct(a.shape, a.dtype) for a in (past_states, past_value, past_key, past_query)),
         in_specs=[hbm] * 5,
-        out_specs=(vmem, hbm, vmem, vmem, vmem),
+        out_specs=(hbm,) * 5,
         scratch_shapes=kept[:4] + [
             pltpu.VMEM(past_states.shape, F32),
             pltpu.VMEM((width, 2 * prop), F32),
-            dma((4,)), dma((own, heads // chunk)), dma((own, heads // chunk)),
+            pltpu.VMEM(past_value.shape, BF16), pltpu.VMEM(past_key.shape, BF16), pltpu.VMEM(past_query.shape, BF16),
+            dma((4,)), dma((own, heads // chunk)), dma((own, heads // chunk)), dma((4,)),
         ],
         compiler_params=pltpu.CompilerParams(vmem_limit_bytes=VMEM_BYTES),
         name="states",

time: 20.6 us -> 20.1 us (0.976)
  Pallas kernels: 19.1 us -> 18.6 us
    pallas_call x1, Pallas kernels: 3.59 us -> 3.03 us  [per_device(): pl.pallas_call(functools.partial(states_kernel, chunk), out_shape=passed[...]
where the time goes in v1:
time: 20.1 us; the launch traced here: 19.9 us
  Pallas kernels  18.6 us (93%)
  between operations  1.29 us (6%)
    pallas_call x1, Pallas kernels, per_device(): pl.pallas_call(functools.partial(mixer_kernel, n_kv, n_tp), out_shape=pas...  15.5 us
    pallas_call x1, Pallas kernels, per_device(): pl.pallas_call(functools.partial(states_kernel, chunk), out_shape=passed[...  3.03 us

profile of v1, /device:TPU:0, one launch (start us, length us, event | category | flops | bytes accessed | tf_op | source)
XLA Modules:
  0.0 19.9 jit_solution(6024207298438522649)
XLA Ops:
  1.3 15.5 %mixer.1 = (bf16[4,4,512]{2,1,0:T(4,128)(2,1)}, f32[1,7,1536]{2,1,0:T(8,128)}, f32[1,8,1024]{2,1,0:T(8,128)}, f32[1,4,256]{2,1,0:T(4,128)}, f32[1,16,64,128]{3,2,1,0:T(8,128)}) custom-call(bf16[4,4,512]{2,1,0:T(4,128)(2,1)} %refs_0_.1, f32[512]{0:T(512)} %refs_1_.1, bf16[512,1024]{1,0:T(8,128)(2,1)} %refs_2_.1, bf16[512,1024]{1,0:T(8,128)(2,1)} %refs_3_.1, ...), custom_call_target="tpu_custom_call" | custom-call | tf_op jit(solution)/shard_map/mixer/pallas_call | solution.py:355
  16.8 3.0 %states.1 = (bf16[4,4,512]{2,1,0:T(4,128)(2,1)}, f32[1,5,16,64,128]{4,3,2,1,0:T(8,128)}, bf16[1,7,1024]{2,1,0:T(8,128)(2,1)}, bf16[1,7,256]{2,1,0:T(8,128)(2,1)}, bf16[1,7,256]{2,1,0:T(8,128)(2,1)}) custom-call(bf16[4,4,512]{2,1,0:T(4,128)(2,1)} %get-tuple-element.10.mixed_h, f32[1,7,1536]{2,1,0:T(8,128)} %get-tuple-element.11.hist_h, ...), custom_call_target="tpu_custom_call" | custom-call | tf_op jit(solution)/shard_map/states/pallas_call | solution.py:385
